TPU v7x, 32 devices: a whole 2x2x4 slice. The times are simulated.
32 devices in a mesh: sp: 4 (over x, core), dp: 8 (over z, y).
Axes of the slice: x: 2, y: 2, z: 4, core: 2. Of those that a mesh axis runs over, the one named last changes fastest.
Arguments:
- tokens: bfloat16 [8, 1536, 2048], P('dp', 'sp'), may hold values from -6 to 6
- w_value: bfloat16 [2048, 1024], P('dp'), may hold values from -0.125 to 0.125
- w_gate: bfloat16 [2048, 1024], P('dp'), may hold values from -0.125 to 0.125
- conv_taps: bfloat16 [31, 1024], replicated, may hold values from -1 to 1
- norm_gain: bfloat16 [1024], replicated, may hold values from 0.099609375 to 1.8984375
- w_out: bfloat16 [1024, 2048], P(None, 'dp'), may hold values from -0.1875 to 0.1875
Outputs:
- mixed: bfloat16 [8, 1536, 2048], P('dp', 'sp')
All inputs are finite; a program needn't handle non-finite values.
Results may differ from a plain program's by a relative error of at most 0.013.
Values may be sent and summed in bfloat16 or wider, within the bound.
No kernel may reach another device: no remote copies, remote signals or barrier semaphores. Data moves between devices by JAX's collectives and lax.ppermute only.
A program may use at most 64 MiB of HBM per device.

v0:
```python
import jax
import jax.numpy as jnp
from jax import lax
from jax.sharding import PartitionSpec as P

EPSILON = 1e-06


def passed_along(x, axis, by):
    length = lax.axis_size(axis)
    pairs = [(i, i + by) for i in range(length) if 0 <= i + by < length]
    return lax.ppermute(x, axis, pairs)


def depthwise_conv(signal, local_taps, left_pad):
    kernel_form = jnp.transpose(local_taps)[:, None, :]
    result = lax.conv_general_dilated(
        signal[None],
        kernel_form,
        (1,),
        [(left_pad, 0)],
        dimension_numbers=("NCH", "OIH", "NCH"),
        feature_group_count=signal.shape[0],
        preferred_element_type=jnp.float32,
    )
    return result[0].astype(jnp.bfloat16)


def body(tokens, w_value, w_gate, conv_taps, norm_gain, w_out):
    seq_rows = tokens[0]
    tok_count = seq_rows.shape[0]
    kernel_len = conv_taps.shape[0]
    value_sum = jnp.einsum(
        "dc,td->ct",
        lax.all_gather(w_value, "dp", axis=0, tiled=True),
        seq_rows,
        preferred_element_type=jnp.float32,
    )
    gate_sum = jnp.einsum(
        "dc,td->ct",
        lax.all_gather(w_gate, "dp", axis=0, tiled=True),
        seq_rows,
        preferred_element_type=jnp.float32,
    )
    gated = (value_sum * jax.nn.sigmoid(gate_sum)).astype(jnp.bfloat16)
    last_rows = gated[:, tok_count - (kernel_len - 1) :]
    earlier = passed_along(last_rows, "sp", 1)
    extended = jnp.concatenate([earlier, gated], axis=1)
    conv_out = depthwise_conv(extended, conv_taps, 0)
    wide = conv_out.astype(jnp.float32)
    chan_mean = jnp.mean(wide, 0, keepdims=True)
    centred = wide - chan_mean
    chan_var = jnp.mean(centred * centred, 0, keepdims=True)
    normed = centred * lax.rsqrt(chan_var + EPSILON) * norm_gain.astype(jnp.float32)[:, None]
    activated = (normed * jax.nn.sigmoid(normed)).astype(jnp.bfloat16)
    projected = jnp.einsum(
        "ct,cd->td",
        activated,
        lax.all_gather(w_out, "dp", axis=1, tiled=True),
        preferred_element_type=jnp.float32,
    ).astype(jnp.bfloat16)
    return projected[None]


def solution(mesh):
    placed = (P("dp", "sp", None), P("dp", None), P("dp", None), P(), P(), P(None, "dp"))
    return jax.shard_map(
        body, mesh=mesh, in_specs=placed, out_specs=P("dp", "sp", None), check_vma=False
    )
```

profile of v0, /device:TPU:0, one launch (start us, length us, event | category | flops | bytes accessed | tf_op | source)
XLA Modules:
  0.0 246.4 jit_solution(6799378059922831921)
XLA Ops:
  6.5 0.0 copy-start
  6.5 0.0 all-gather.6.cloned.1.call-start
  6.5 0.7 all-gather.6.cloned.1.call-update
  7.3 0.0 all-gather.4.cloned.1.call-start
  7.3 0.7 all-gather.4.cloned.1.call-update
  8.0 0.0 all-gather.8.cloned.1.call-start
  8.1 0.7 all-gather.8.cloned.1.call-update
  8.7 76.3 %all-gather.6.cloned.1.call-done = bf16[2048,1024]{1,0:T(8,128)(2,1)} async-done(((bf16[256,1024]{1,0:T(8,128)(2,1)}), bf16[2048,1024]{1,0:T(8,128)(2,1)}) %all-gather.6.cloned.1.call-update) | async-done | bytes 4194320 | tf_op jit(solution)/shard_map/all_gather | solution.py:41
  85.0 0.0 copy-done
  85.0 4.0 %fusion.4 = f32[1024,384]{0,1:T(8,128)S(1)} fusion(bf16[2048,1024]{1,0:T(8,128)(2,1)} %all-gather.6.cloned.1.call-done, bf16[1,384,2048]{2,1,0:T(8,128)(2,1)S(1)} %copy-done), kind=kOutput, calls=%fused_computation.8 | convolution fusion | flops 1610612736 | bytes 7340032 | tf_op jit(solution)/shard_map/dc,td->ct/dot_general | solution.py:39
  89.0 0.0 copy-start.1
  89.0 69.5 %all-gather.4.cloned.1.call-done = bf16[2048,1024]{1,0:T(8,128)(2,1)} async-done(((bf16[256,1024]{1,0:T(8,128)(2,1)}), bf16[2048,1024]{1,0:T(8,128)(2,1)}) %all-gather.4.cloned.1.call-update) | async-done | bytes 4194320 | tf_op jit(solution)/shard_map/all_gather | solution.py:35
  158.5 4.1 %multiply_convert_fusion.1 = bf16[1024,384]{0,1:T(8,128)(2,1)S(1)} fusion(f32[1024,384]{0,1:T(8,128)S(1)} %fusion.4, bf16[2048,1024]{1,0:T(8,128)(2,1)} %all-gather.4.cloned.1.call-done, bf16[1,384,2048]{2,1,0:T(8,128)(2,1)S(1)} %copy-done), kind=kOutput, calls=%fused_computation.12 | convolution fusion | flops 1612578816 | bytes 8126464 | tf_op jit(solution)/shard_map/dc,td->ct/dot_general | solution.py:33
  162.6 1.3 collective-permute-start
  163.9 0.0 copy-done.1
  163.9 0.9 collective-permute-done
  164.8 0.2 maximum_bitcast_fusion
  165.0 0.1 pad
  165.0 0.2 reshape.17
  165.2 0.0 copy-start.2
  165.2 0.0 copy-start.3
  165.2 0.5 copy.12
  165.7 0.1 slice.7
  165.8 0.2 copy-done.2
  166.0 0.0 copy-done.3
  166.0 3.8 %fusion.17 = f32[8,52,1024]{2,0,1:T(8,128)S(1)} fusion(bf16[1024,1,7,30]{0,2,3,1:T(8,128)(2,1)S(1)} %slice.7, bf16[1024,1,8,52]{0,2,3,1:T(8,128)(2,1)S(1)} %copy.12, pred[8,52]{0,1:T(8,128)(4,1)S(1)} %copy-done.3, bf16[1024,1,31]{0,2,1:T(8,128)(2,1)S(1)} %bitcast.35), kind=kOutput, calls=%fused_computation.20 | convolution fusion | flops 31719424 | bytes 3049888 | tf_op jit(solution)/shard_map/conv_general_dilated | solution.py:17
  169.8 2.2 copy.14
  172.1 1.6 reshape.21
  173.7 0.2 slice_reduce_fusion
  173.8 0.3 multiply_reduce_fusion
  174.1 60.3 %all-gather.8.cloned.1.call-done = bf16[1024,2048]{1,0:T(8,128)(2,1)} async-done(((bf16[1024,256]{1,0:T(8,128)(2,1)}), bf16[1024,2048]{1,0:T(8,128)(2,1)}) %all-gather.8.cloned.1.call-update) | async-done | bytes 4194320 | tf_op jit(solution)/shard_map/all_gather | solution.py:59
  234.5 5.5 %fusion.1 = bf16[1,384,2048]{2,1,0:T(8,128)(2,1)} fusion(bf16[1024,2048]{1,0:T(8,128)(2,1)} %all-gather.8.cloned.1.call-done, f32[1,416,1024]{2,1,0:T(8,128)S(1)} %reshape.21, f32[1024]{0:T(1024)S(1)} %convert_element_type.26, f32[384]{0:T(512)S(1)} %add_rsqrt_fusion, f32[384]{0:T(512)S(1)} %broadcast_multiply_fusion), kind=kOutput, calls=%fused_computation.3 | convolution fusion | flops 1614544896 | bytes 7348224 | tf_op jit(solution)/shard_map/ct,cd->td/dot_general | solution.py:56
  (4 shorter events, 0.0 us)
Async XLA Ops:
  6.5 78.5 %copy-start = (bf16[1,384,2048]{2,1,0:T(8,128)(2,1)S(1)}, bf16[1,384,2048]{2,1,0:T(8,128)(2,1)}, u32[]{:S(2)}) copy-start(bf16[1,384,2048]{2,1,0:T(8,128)(2,1)} %param.6) | copy-start | bytes 4718596
  6.5 78.5 %all-gather.6.cloned.1.call-start = ((), (), s32[]{:S(2)}) async-start(), calls=%async_computation.1 | async-start | bytes 4718592 | tf_op jit(solution)/shard_map/all_gather | solution.py:41
  7.3 151.2 %all-gather.4.cloned.1.call-start = ((), (), s32[]{:S(2)}) async-start(), calls=%async_computation | async-start | bytes 4718592 | tf_op jit(solution)/shard_map/all_gather | solution.py:35
  8.0 226.4 %all-gather.8.cloned.1.call-start = ((), (), s32[]{:S(2)}) async-start(), calls=%async_computation.2 | async-start | bytes 4718592 | tf_op jit(solution)/shard_map/all_gather | solution.py:59
  89.0 74.9 %copy-start.1 = (bf16[1024]{0:T(1024)(128)(2,1)S(1)}, bf16[1024]{0:T(1024)(128)(2,1)}, u32[]{:S(2)}) copy-start(bf16[1024]{0:T(1024)(128)(2,1)} %param.10) | copy-start | bytes 6148
  162.6 2.2 collective-permute-start
  165.2 0.8 copy-start.2
  165.2 0.8 copy-start.3
Sparse Core Ops, SparseCore 0:
  9.5 75.5 all-gather.5
  87.1 71.3 all-gather.3
  160.5 73.8 all-gather.7
where the time goes:
time: 247 us; the launch traced here: 246 us
  waiting for transfers between devices  209 us (85%)
  matrix products  17.3 us (7%)
  between operations  13.2 us (5%)
  local copies, waits for them, and re-layouts  4.87 us (2%)
    all_gather x1, waiting for transfers between devices, body(): lax.all_gather(w_gate, 'dp', axis=0, tiled=True)  76.3 us
    all_gather x1, waiting for transfers between devices, body(): lax.all_gather(w_value, 'dp', axis=0, tiled=True)  69.5 us
    all_gather x1, waiting for transfers between devices, body(): lax.all_gather(w_out, 'dp', axis=1, tiled=True)  60.3 us
    dot_general x1, matrix products, body(): jnp.einsum('ct,cd->td', activated, lax.all_gather(w_out, 'dp', axis=1, ti...  5.46 us
  transfers between devices with their start and end apart: 4, of which 4 were waited for; matrix products, arithmetic and copies ran while one was open for 7% of the time, Pallas kernels for 0%

commit v1 on v0

--- a/solution.py
+++ b/solution.py
@@ -30,12 +30,27 @@
     seq_rows = tokens[0]
     tok_count = seq_rows.shape[0]
     kernel_len = conv_taps.shape[0]
+    v1 = lax.axis_size("dp")
+    inter, w1 = (v1, lax.axis_index("dp"))
+    gallery = []
+    for num in [*range(inter)]:
+        gallery.append((num, (num - 1) % inter))
+    local_now = w_value.shape[0]
+    res = w_value
     value_sum = jnp.einsum(
         "dc,td->ct",
-        lax.all_gather(w_value, "dp", axis=0, tiled=True),
-        seq_rows,
+        res,
+        lax.dynamic_slice_in_dim(seq_rows, w1 * local_now, res.shape[0], axis=1),
         preferred_element_type=jnp.float32,
     )
+    for k in [*range(1, inter)]:
+        res = lax.ppermute(res, "dp", gallery)
+        value_sum = value_sum + jnp.einsum(
+            "dc,td->ct",
+            res,
+            lax.dynamic_slice_in_dim(seq_rows, (w1 + k) % inter * local_now, res.shape[0], axis=1),
+            preferred_element_type=jnp.float32,
+        )
     gate_sum = jnp.einsum(
         "dc,td->ct",
         lax.all_gather(w_gate, "dp", axis=0, tiled=True),

time: 247 us -> 226 us (0.915)
  waiting for transfers between devices: 209 us -> 139 us
  starting transfers between devices: 1.37 us -> 38.8 us
  matrix products: 17.3 us -> 28 us
    ppermute x0 -> x7, waiting for transfers between devices: none -> 101 us  [body(): res = lax.ppermute(res, 'dp', gallery)]
    all_gather x1, waiting for transfers between devices: 76.3 us -> 0.01 us  [body(): lax.all_gather(w_gate, 'dp', axis=0, tiled=True)]
    all_gather x1 -> x0, waiting for transfers between devices: 69.5 us -> none  [body(): lax.all_gather(w_value, 'dp', axis=0, tiled=True)]
    ppermute x0 -> x7, starting transfers between devices: none -> 37.2 us  [body(): res = lax.ppermute(res, 'dp', gallery)]
    all_gather x1, waiting for transfers between devices: 60.3 us -> 36.5 us  [body(): lax.all_gather(w_out, 'dp', axis=1, tiled=True)]
    dot_general x1 -> x8, matrix products: 4.05 us -> 14.6 us  [the longest x7 13.2 us: body(): jnp.einsum('dc,td->ct', res, lax.dynamic_slice_in_dim(seq_rows, (w1 + k)...]
  transfers between devices with their start and end apart: 4 -> 10, of which waited for: 4 -> 9; matrix products, arithmetic and copies ran while one was open for 7% -> 12% of each run, Pallas kernels for 0% -> 0%
where the time goes in v1:
time: 226 us; the launch traced here: 225 us
  waiting for transfers between devices  139 us (62%)
  starting transfers between devices  38.8 us (17%)
  matrix products  28 us (12%)
  between operations  13.6 us (6%)
  local copies, waits for them, and re-layouts  4.94 us (2%)
    ppermute x7, waiting for transfers between devices, body(): res = lax.ppermute(res, 'dp', gallery)  101 us
    ppermute x7, starting transfers between devices, body(): res = lax.ppermute(res, 'dp', gallery)  37.2 us
    all_gather x1, waiting for transfers between devices, body(): lax.all_gather(w_out, 'dp', axis=1, tiled=True)  36.5 us
    dot_general x7, matrix products, body(): jnp.einsum('dc,td->ct', res, lax.dynamic_slice_in_dim(seq_rows, (w1 + k)...  13.2 us
    dot_general x1, matrix products, body(): jnp.einsum('ct,cd->td', activated, lax.all_gather(w_out, 'dp', axis=1, ti...  5.43 us
  transfers between devices with their start and end apart: 10, of which 9 were waited for; matrix products, arithmetic and copies ran while one was open for 12% of the time, Pallas kernels for 0%

profile of v1, /device:TPU:0, one launch (start us, length us, event | category | flops | bytes accessed | tf_op | source)
XLA Modules:
  0.0 225.2 jit_solution(10830962315625716754)
XLA Ops:
  6.5 0.0 all-gather.3.cloned.1.call-start
  6.5 0.7 all-gather.3.cloned.1.call-update
  7.3 0.0 all-gather.5.cloned.1.call-start
  7.3 0.7 all-gather.5.cloned.1.call-update
  8.0 6.1 %collective-permute-start = (bf16[256,1024]{1,0:T(8,128)(2,1)}, bf16[256,1024]{1,0:T(8,128)(2,1)S(1)}, u32[]{:S(2)}, u32[]{:S(2)}) collective-permute-start(bf16[256,1024]{1,0:T(8,128)(2,1)} %param.7), channel_id=1, source_target_pairs={{0,7},{1,0},{2,1},{3,2},{4,3},{5,4},{6,5},{7,6},{8,15},{9,8},{10,9... | collective-permute-start | bytes 1572872 | tf_op jit(solution)/shard_map/ppermute | solution.py:47
  14.1 17.0 %collective-permute-done = bf16[256,1024]{1,0:T(8,128)(2,1)S(1)} collective-permute-done((bf16[256,1024]{1,0:T(8,128)(2,1)}, bf16[256,1024]{1,0:T(8,128)(2,1)S(1)}, u32[]{:S(2)}, u32[]{:S(2)}) %collective-permute-start) | collective-permute-done | bytes 524320 | tf_op jit(solution)/shard_map/ppermute | solution.py:47
  31.1 5.1 %collective-permute-start.1 = (bf16[256,1024]{1,0:T(8,128)(2,1)S(1)}, bf16[256,1024]{1,0:T(8,128)(2,1)S(1)}, u32[]{:S(2)}, u32[]{:S(2)}) collective-permute-start(bf16[256,1024]{1,0:T(8,128)(2,1)S(1)} %collective-permute-done), channel_id=1, source_target_pairs={{0,7},{1,0},{2,1},{3,2},{4,3},{5,4},{6,5},{7,6},{8,15},{9,8},{10,9... | collective-permute-start | bytes 1572872 | tf_op jit(solution)/shard_map/ppermute | solution.py:47
  36.2 17.4 %collective-permute-done.1 = bf16[256,1024]{1,0:T(8,128)(2,1)S(1)} collective-permute-done((bf16[256,1024]{1,0:T(8,128)(2,1)S(1)}, bf16[256,1024]{1,0:T(8,128)(2,1)S(1)}, u32[]{:S(2)}, u32[]{:S(2)}) %collective-permute-start.1) | collective-permute-done | bytes 524320 | tf_op jit(solution)/shard_map/ppermute | solution.py:47
  53.6 5.2 %collective-permute-start.2 = (bf16[256,1024]{1,0:T(8,128)(2,1)S(1)}, bf16[256,1024]{1,0:T(8,128)(2,1)}, u32[]{:S(2)}, u32[]{:S(2)}) collective-permute-start(bf16[256,1024]{1,0:T(8,128)(2,1)S(1)} %collective-permute-done.1), channel_id=1, source_target_pairs={{0,7},{1,0},{2,1},{3,2},{4,3},{5,4},{6,5},{7,6},{8,15},{9,8},{10,9... | collective-permute-start | bytes 1572872 | tf_op jit(solution)/shard_map/ppermute | solution.py:47
  58.8 21.3 %collective-permute-done.2 = bf16[256,1024]{1,0:T(8,128)(2,1)} collective-permute-done((bf16[256,1024]{1,0:T(8,128)(2,1)S(1)}, bf16[256,1024]{1,0:T(8,128)(2,1)}, u32[]{:S(2)}, u32[]{:S(2)}) %collective-permute-start.2) | collective-permute-done | bytes 524320 | tf_op jit(solution)/shard_map/ppermute | solution.py:47
  80.1 0.0 copy-done.7
  80.1 5.3 %collective-permute-start.3 = (bf16[256,1024]{1,0:T(8,128)(2,1)}, bf16[256,1024]{1,0:T(8,128)(2,1)S(1)}, u32[]{:S(2)}, u32[]{:S(2)}) collective-permute-start(bf16[256,1024]{1,0:T(8,128)(2,1)} %collective-permute-done.2), channel_id=1, source_target_pairs={{0,7},{1,0},{2,1},{3,2},{4,3},{5,4},{6,5},{7,6},{8,15},{9,8},{10,9... | collective-permute-start | bytes 1572872 | tf_op jit(solution)/shard_map/ppermute | solution.py:47
  85.4 1.4 fusion.35
  86.8 0.0 copy-start.8
  86.8 1.6 fusion.33
  88.5 19.0 %collective-permute-done.3 = bf16[256,1024]{1,0:T(8,128)(2,1)S(1)} collective-permute-done((bf16[256,1024]{1,0:T(8,128)(2,1)}, bf16[256,1024]{1,0:T(8,128)(2,1)S(1)}, u32[]{:S(2)}, u32[]{:S(2)}) %collective-permute-start.3) | collective-permute-done | bytes 524320 | tf_op jit(solution)/shard_map/ppermute | solution.py:47
  107.5 5.1 %collective-permute-start.4 = (bf16[256,1024]{1,0:T(8,128)(2,1)S(1)}, bf16[256,1024]{1,0:T(8,128)(2,1)S(1)}, u32[]{:S(2)}, u32[]{:S(2)}) collective-permute-start(bf16[256,1024]{1,0:T(8,128)(2,1)S(1)} %collective-permute-done.3), channel_id=1, source_target_pairs={{0,7},{1,0},{2,1},{3,2},{4,3},{5,4},{6,5},{7,6},{8,15},{9,8},{10,9... | collective-permute-start | bytes 1572872 | tf_op jit(solution)/shard_map/ppermute | solution.py:47
  112.5 1.5 fusion.31
  114.1 2.6 %fusion.29 = f32[384,1024]{1,0:T(8,128)} fusion(bf16[256,1024]{1,0:T(8,128)(2,1)} %collective-permute-done.2, bf16[1,384,2048]{2,1,0:T(8,128)(2,1)S(1)} %copy-done, s32[]{:T(128)S(6)} %select_n.61), kind=kOutput, calls=%fused_computation.33 | convolution fusion | flops 201326592 | bytes 2293764 | tf_op jit(solution)/shard_map/dc,td->ct/dot_general | solution.py:48
  116.7 8.4 %collective-permute-done.4 = bf16[256,1024]{1,0:T(8,128)(2,1)S(1)} collective-permute-done((bf16[256,1024]{1,0:T(8,128)(2,1)S(1)}, bf16[256,1024]{1,0:T(8,128)(2,1)S(1)}, u32[]{:S(2)}, u32[]{:S(2)}) %collective-permute-start.4) | collective-permute-done | bytes 524320 | tf_op jit(solution)/shard_map/ppermute | solution.py:47
  125.1 5.2 %collective-permute-start.5 = (bf16[256,1024]{1,0:T(8,128)(2,1)S(1)}, bf16[256,1024]{1,0:T(8,128)(2,1)}, u32[]{:S(2)}, u32[]{:S(2)}) collective-permute-start(bf16[256,1024]{1,0:T(8,128)(2,1)S(1)} %collective-permute-done.4), channel_id=1, source_target_pairs={{0,7},{1,0},{2,1},{3,2},{4,3},{5,4},{6,5},{7,6},{8,15},{9,8},{10,9... | collective-permute-start | bytes 1572872 | tf_op jit(solution)/shard_map/ppermute | solution.py:47
  130.2 1.5 fusion.27
  131.8 1.5 fusion.25
  133.3 11.0 %collective-permute-done.5 = bf16[256,1024]{1,0:T(8,128)(2,1)} collective-permute-done((bf16[256,1024]{1,0:T(8,128)(2,1)S(1)}, bf16[256,1024]{1,0:T(8,128)(2,1)}, u32[]{:S(2)}, u32[]{:S(2)}) %collective-permute-start.5) | collective-permute-done | bytes 524320 | tf_op jit(solution)/shard_map/ppermute | solution.py:47
  144.3 5.3 %collective-permute-start.6 = (bf16[256,1024]{1,0:T(8,128)(2,1)}, bf16[256,1024]{1,0:T(8,128)(2,1)}, u32[]{:S(2)}, u32[]{:S(2)}) collective-permute-start(bf16[256,1024]{1,0:T(8,128)(2,1)} %collective-permute-done.5), channel_id=1, source_target_pairs={{0,7},{1,0},{2,1},{3,2},{4,3},{5,4},{6,5},{7,6},{8,15},{9,8},{10,9... | collective-permute-start | bytes 1572872 | tf_op jit(solution)/shard_map/ppermute | solution.py:47
  149.7 2.6 %fusion.23 = f32[384,1024]{1,0:T(8,128)} fusion(bf16[256,1024]{1,0:T(8,128)(2,1)} %collective-permute-done.5, bf16[1,384,2048]{2,1,0:T(8,128)(2,1)S(1)} %copy-done, s32[]{:T(128)S(6)} %select_n.67), kind=kOutput, calls=%fused_computation.27 | convolution fusion | flops 201326592 | bytes 2293764 | tf_op jit(solution)/shard_map/dc,td->ct/dot_general | solution.py:48
  152.3 0.0 copy-start.6
  152.3 4.1 %fusion.2 = f32[1024,384]{0,1:T(8,128)S(1)} fusion(bf16[2048,1024]{1,0:T(8,128)(2,1)} %all-gather.3.cloned.1.call-done, bf16[1,384,2048]{2,1,0:T(8,128)(2,1)S(1)} %copy-done), kind=kOutput, calls=%fused_computation.6 | convolution fusion | flops 1610612736 | bytes 7340032 | tf_op jit(solution)/shard_map/dc,td->ct/dot_general | solution.py:54
  156.4 0.0 copy-start.11
  156.4 6.6 %collective-permute-done.6 = bf16[256,1024]{1,0:T(8,128)(2,1)} collective-permute-done((bf16[256,1024]{1,0:T(8,128)(2,1)}, bf16[256,1024]{1,0:T(8,128)(2,1)}, u32[]{:S(2)}, u32[]{:S(2)}) %collective-permute-start.6) | collective-permute-done | bytes 524320 | tf_op jit(solution)/shard_map/ppermute | solution.py:47
  163.0 1.8 fusion.4
  164.9 1.5 collective-permute-start.7
  166.4 0.7 collective-permute-done.7
  167.1 0.2 maximum_bitcast_fusion
  167.3 0.1 pad
  167.4 0.2 reshape.25
  167.5 0.0 copy-start.12
  167.5 0.0 copy-start.13
  167.5 0.5 copy.12
  168.0 0.1 slice.7
  168.1 0.2 copy-done.12
  168.4 3.8 %fusion.14 = f32[8,52,1024]{2,0,1:T(8,128)S(1)} fusion(bf16[1024,1,7,30]{0,2,3,1:T(8,128)(2,1)S(1)} %slice.7, bf16[1024,1,8,52]{0,2,3,1:T(8,128)(2,1)S(1)} %copy.12, pred[8,52]{0,1:T(8,128)(4,1)S(1)} %copy-done.13, bf16[1024,1,31]{0,2,1:T(8,128)(2,1)S(1)} %bitcast.66), kind=kOutput, calls=%fused_computation.19 | convolution fusion | flops 31719424 | bytes 3049888 | tf_op jit(solution)/shard_map/conv_general_dilated | solution.py:17
  172.2 2.2 copy.14
  174.4 1.6 reshape.29
  176.0 0.2 slice_reduce_fusion
  176.2 0.3 multiply_reduce_fusion
  176.5 36.5 %all-gather.5.cloned.1.call-done = bf16[1024,2048]{1,0:T(8,128)(2,1)} async-done(((bf16[1024,256]{1,0:T(8,128)(2,1)}), bf16[1024,2048]{1,0:T(8,128)(2,1)}) %all-gather.5.cloned.1.call-update) | async-done | bytes 4194320 | tf_op jit(solution)/shard_map/all_gather | solution.py:74
  212.9 5.4 %fusion.1 = bf16[1,384,2048]{2,1,0:T(8,128)(2,1)} fusion(bf16[1024,2048]{1,0:T(8,128)(2,1)} %all-gather.5.cloned.1.call-done, f32[1,416,1024]{2,1,0:T(8,128)S(1)} %reshape.29, f32[1024]{0:T(1024)S(1)} %convert_element_type.26, f32[384]{0:T(512)S(1)} %add_rsqrt_fusion, f32[384]{0:T(512)S(1)} %broadcast_multiply_fusion), kind=kOutput, calls=%fused_computation.3 | convolution fusion | flops 1614544896 | bytes 7348224 | tf_op jit(solution)/shard_map/ct,cd->td/dot_general | solution.py:71
  (26 shorter events, 0.1 us)
Async XLA Ops:
  6.5 78.9 %copy-start = (bf16[1,384,2048]{2,1,0:T(8,128)(2,1)S(1)}, bf16[1,384,2048]{2,1,0:T(8,128)(2,1)}, u32[]{:S(2)}) copy-start(bf16[1,384,2048]{2,1,0:T(8,128)(2,1)} %param.6) | copy-start | bytes 4718596
  6.5 145.7 %all-gather.3.cloned.1.call-start = ((), (), s32[]{:S(2)}) async-start(), calls=%async_computation | async-start | bytes 4718592 | tf_op jit(solution)/shard_map/all_gather | solution.py:56
  7.3 205.7 %all-gather.5.cloned.1.call-start = ((), (), s32[]{:S(2)}) async-start(), calls=%async_computation.1 | async-start | bytes 4718592 | tf_op jit(solution)/shard_map/all_gather | solution.py:74
  8.0 23.1 %collective-permute-start = (bf16[256,1024]{1,0:T(8,128)(2,1)}, bf16[256,1024]{1,0:T(8,128)(2,1)S(1)}, u32[]{:S(2)}, u32[]{:S(2)}) collective-permute-start(bf16[256,1024]{1,0:T(8,128)(2,1)} %param.7), channel_id=1, source_target_pairs={{0,7},{1,0},{2,1},{3,2},{4,3},{5,4},{6,5},{7,6},{8,15},{9,8},{10,9... | collective-permute-start | bytes 1572872 | tf_op jit(solution)/shard_map/ppermute | solution.py:47
  31.1 22.5 %copy-start.9 = (bf16[256,1024]{1,0:T(8,128)(2,1)}, bf16[256,1024]{1,0:T(8,128)(2,1)S(1)}, u32[]{:S(2)}) copy-start(bf16[256,1024]{1,0:T(8,128)(2,1)S(1)} %collective-permute-done) | copy-start | bytes 1572868
  31.1 22.5 %collective-permute-start.1 = (bf16[256,1024]{1,0:T(8,128)(2,1)S(1)}, bf16[256,1024]{1,0:T(8,128)(2,1)S(1)}, u32[]{:S(2)}, u32[]{:S(2)}) collective-permute-start(bf16[256,1024]{1,0:T(8,128)(2,1)S(1)} %collective-permute-done), channel_id=1, source_target_pairs={{0,7},{1,0},{2,1},{3,2},{4,3},{5,4},{6,5},{7,6},{8,15},{9,8},{10,9... | collective-permute-start | bytes 1572872 | tf_op jit(solution)/shard_map/ppermute | solution.py:47
  53.6 26.5 %copy-start.7 = (bf16[256,1024]{1,0:T(8,128)(2,1)}, bf16[256,1024]{1,0:T(8,128)(2,1)S(1)}, u32[]{:S(2)}) copy-start(bf16[256,1024]{1,0:T(8,128)(2,1)S(1)} %collective-permute-done.1) | copy-start | bytes 1572868
  53.6 26.5 %collective-permute-start.2 = (bf16[256,1024]{1,0:T(8,128)(2,1)S(1)}, bf16[256,1024]{1,0:T(8,128)(2,1)}, u32[]{:S(2)}, u32[]{:S(2)}) collective-permute-start(bf16[256,1024]{1,0:T(8,128)(2,1)S(1)} %collective-permute-done.1), channel_id=1, source_target_pairs={{0,7},{1,0},{2,1},{3,2},{4,3},{5,4},{6,5},{7,6},{8,15},{9,8},{10,9... | collective-permute-start | bytes 1572872 | tf_op jit(solution)/shard_map/ppermute | solution.py:47
  58.8 28.1 %copy-start.10 = (bf16[256,1024]{1,0:T(8,128)(2,1)S(1)}, bf16[256,1024]{1,0:T(8,128)(2,1)}, u32[]{:S(2)}) copy-start(bf16[256,1024]{1,0:T(8,128)(2,1)} %copy-done.9) | copy-start | bytes 1572868
  80.1 27.4 %collective-permute-start.3 = (bf16[256,1024]{1,0:T(8,128)(2,1)}, bf16[256,1024]{1,0:T(8,128)(2,1)S(1)}, u32[]{:S(2)}, u32[]{:S(2)}) collective-permute-start(bf16[256,1024]{1,0:T(8,128)(2,1)} %collective-permute-done.2), channel_id=1, source_target_pairs={{0,7},{1,0},{2,1},{3,2},{4,3},{5,4},{6,5},{7,6},{8,15},{9,8},{10,9... | collective-permute-start | bytes 1572872 | tf_op jit(solution)/shard_map/ppermute | solution.py:47
  86.8 25.7 %copy-start.8 = (bf16[256,1024]{1,0:T(8,128)(2,1)S(1)}, bf16[256,1024]{1,0:T(8,128)(2,1)}, u32[]{:S(2)}) copy-start(bf16[256,1024]{1,0:T(8,128)(2,1)} %copy-done.7) | copy-start | bytes 1572868
  107.5 17.6 %collective-permute-start.4 = (bf16[256,1024]{1,0:T(8,128)(2,1)S(1)}, bf16[256,1024]{1,0:T(8,128)(2,1)S(1)}, u32[]{:S(2)}, u32[]{:S(2)}) collective-permute-start(bf16[256,1024]{1,0:T(8,128)(2,1)S(1)} %collective-permute-done.3), channel_id=1, source_target_pairs={{0,7},{1,0},{2,1},{3,2},{4,3},{5,4},{6,5},{7,6},{8,15},{9,8},{10,9... | collective-permute-start | bytes 1572872 | tf_op jit(solution)/shard_map/ppermute | solution.py:47
  125.1 19.3 %collective-permute-start.5 = (bf16[256,1024]{1,0:T(8,128)(2,1)S(1)}, bf16[256,1024]{1,0:T(8,128)(2,1)}, u32[]{:S(2)}, u32[]{:S(2)}) collective-permute-start(bf16[256,1024]{1,0:T(8,128)(2,1)S(1)} %collective-permute-done.4), channel_id=1, source_target_pairs={{0,7},{1,0},{2,1},{3,2},{4,3},{5,4},{6,5},{7,6},{8,15},{9,8},{10,9... | collective-permute-start | bytes 1572872 | tf_op jit(solution)/shard_map/ppermute | solution.py:47
  144.3 18.7 %collective-permute-start.6 = (bf16[256,1024]{1,0:T(8,128)(2,1)}, bf16[256,1024]{1,0:T(8,128)(2,1)}, u32[]{:S(2)}, u32[]{:S(2)}) collective-permute-start(bf16[256,1024]{1,0:T(8,128)(2,1)} %collective-permute-done.5), channel_id=1, source_target_pairs={{0,7},{1,0},{2,1},{3,2},{4,3},{5,4},{6,5},{7,6},{8,15},{9,8},{10,9... | collective-permute-start | bytes 1572872 | tf_op jit(solution)/shard_map/ppermute | solution.py:47
  152.3 10.7 %copy-start.1 = (f32[384,1024]{1,0:T(8,128)S(1)}, f32[384,1024]{1,0:T(8,128)}, u32[]{:S(2)}) copy-start(f32[384,1024]{1,0:T(8,128)} %fusion.33) | copy-start | bytes 4718596
  152.3 10.7 %copy-start.2 = (f32[384,1024]{1,0:T(8,128)S(1)}, f32[384,1024]{1,0:T(8,128)}, u32[]{:S(2)}) copy-start(f32[384,1024]{1,0:T(8,128)} %fusion.31) | copy-start | bytes 4718596
  152.3 10.7 %copy-start.3 = (f32[384,1024]{1,0:T(8,128)S(1)}, f32[384,1024]{1,0:T(8,128)}, u32[]{:S(2)}) copy-start(f32[384,1024]{1,0:T(8,128)} %fusion.29) | copy-start | bytes 4718596
  152.3 10.7 %copy-start.4 = (f32[384,1024]{1,0:T(8,128)S(1)}, f32[384,1024]{1,0:T(8,128)}, u32[]{:S(2)}) copy-start(f32[384,1024]{1,0:T(8,128)} %fusion.27) | copy-start | bytes 4718596
  152.3 10.7 %copy-start.5 = (f32[384,1024]{1,0:T(8,128)S(1)}, f32[384,1024]{1,0:T(8,128)}, u32[]{:S(2)}) copy-start(f32[384,1024]{1,0:T(8,128)} %fusion.25) | copy-start | bytes 4718596
  152.3 10.7 %copy-start.6 = (f32[384,1024]{1,0:T(8,128)S(1)}, f32[384,1024]{1,0:T(8,128)}, u32[]{:S(2)}) copy-start(f32[384,1024]{1,0:T(8,128)} %fusion.23) | copy-start | bytes 4718596
  156.4 9.9 %copy-start.11 = (bf16[1024]{0:T(1024)(128)(2,1)S(1)}, bf16[1024]{0:T(1024)(128)(2,1)}, u32[]{:S(2)}) copy-start(bf16[1024]{0:T(1024)(128)(2,1)} %param.10) | copy-start | bytes 6148
  164.9 2.2 collective-permute-start.7
  167.5 0.8 copy-start.12
  167.5 0.8 copy-start.13
Sparse Core Ops, SparseCore 0:
  9.5 110.3 all-gather.2
  121.9 91.0 all-gather.4
